TPU v7x, 32 devices: a whole 2x2x4 slice. The times are simulated.
32 devices in a mesh: kv: 8 (over z, y), tp: 4 (over x, core).
Axes of the slice: x: 2, y: 2, z: 4, core: 2. Of those that a mesh axis runs over, the one named last changes fastest.
Arguments:
- tokens: bfloat16 [128, 4096], P(None, 'kv'), may hold values from -152 to 152, as said below
- norm_gain: float32 [4096], P('kv'), may hold values from 0.1 to 1.9
- w_query: bfloat16 [4096, 2048], P('kv', 'tp'), may hold values from -0.09375 to 0.09375
- w_key: bfloat16 [4096, 2048], P('kv', 'tp'), may hold values from -0.375 to 0.375
- w_value: bfloat16 [4096, 2048], P('kv', 'tp'), may hold values from -0.09375 to 0.09375
- lambdas: float32 [16], P('tp'), may hold values from 0.3 to 0.8
- head_gain: float32 [128], replicated, may hold values from 0.1 to 1.9
- w_out: bfloat16 [2048, 4096], P('tp', 'kv'), may hold values from -0.125 to 0.125
- cache_keys: bfloat16 [8, 4096, 16, 128], P(None, 'kv', 'tp'), may hold values from -370 to 370
- cache_values: bfloat16 [8, 4096, 16, 128], P(None, 'kv', 'tp'), may hold values from -6 to 6
- lengths: int32 [8], replicated, may hold values from 2560 to 4074
- accepted: int32 [8], replicated, may hold values from 0 to 6
- parents: int32 [8, 16], replicated, may hold values from -1 to 14, as said below
Outputs:
- layer_out: bfloat16 [128, 4096], P('tp', 'kv')
- keys_out: bfloat16 [8, 4096, 16, 128], P(None, 'kv', 'tp')
- values_out: bfloat16 [8, 4096, 16, 128], P(None, 'kv', 'tp')
Inputs may be any that keep to these rules, and one draw needn't show every extreme that they name: `tokens`: columns of features have scales that differ; rows too. The proposals of the last step that were kept already stand right after the first lengths positions; the next 16 positions receive this step's proposals. `parents`: proposal 0 of every sequence has parent -1; every other proposal's parent is an earlier proposal of the same sequence, and the last proposal's parent is the one right before it.
All inputs are finite; a program needn't handle non-finite values.
Results may differ from a plain program's by a relative error of at most 0.015.
The roundings to bfloat16 on the way count: a program that leaves them out, or rounds other values in their place, can miss the bound.
Values may be sent and summed in bfloat16 or wider, within the bound.
A program may use at most 64 MiB of HBM per device.

v0:
```python
import jax
import jax.numpy as jnp
from jax import lax
from jax.sharding import PartitionSpec as P

D = 4096
HEAD = 64
KDIM = 128
PROP = 16
eps_row = 1e-06
eps_head = 1e-05
masked = -1e30


def ancestry(parents):
    members = parents.shape[0]
    indices = jnp.arange(members, dtype=jnp.int32)
    reachable = (parents[:, None] == indices[None, :]).astype(jnp.float32) + jnp.eye(
        members, dtype=jnp.float32
    )
    for repeat in range(max(1, (members - 1).bit_length())):
        reachable = jnp.minimum(jnp.dot(reachable, reachable, precision=lax.Precision.HIGHEST), 1.0)
    return reachable


def combine(earlier, latter):
    maxima_a, totals_a, summed_a = earlier
    maxima_b, totals_b, summed_b = latter
    highest = jnp.maximum(maxima_a, maxima_b)
    factor_a = jnp.exp(maxima_a - highest)
    factor_b = jnp.exp(maxima_b - highest)
    return (
        highest,
        totals_a * factor_a + totals_b * factor_b,
        summed_a * factor_a[..., None] + summed_b * factor_b[..., None],
    )


def softmax_block(scores, allowed, values):
    scores = jnp.where(allowed, scores, masked)
    maxima = jnp.max(scores, axis=-1)
    weights = jnp.where(allowed, jnp.exp(scores - maxima[..., None]), 0.0)
    totals = jnp.sum(weights, axis=-1)
    summed = jnp.einsum(
        "bjhmp,bphd->bjhmd",
        weights.astype(jnp.bfloat16),
        values,
        preferred_element_type=jnp.float32,
    )
    return (maxima, totals, summed)


def finish(merged, lambdas, head_gain):
    maxima, totals, summed = merged
    attended = summed / totals[..., None]
    blended = attended[..., 0, :] - lambdas[:, None] * attended[..., 1, :]
    inverse_rms = lax.rsqrt(jnp.mean(blended * blended, axis=-1, keepdims=True) + eps_head)
    return (blended * inverse_rms * head_gain).astype(jnp.bfloat16)


def leading(array, token_count):
    return array.reshape((1, token_count) + array.shape[2:])


def body(
    tokens,
    norm_gain,
    w_query,
    w_key,
    w_value,
    lambdas,
    head_gain,
    w_out,
    cache_keys,
    cache_values,
    lengths,
    accepted,
    parents,
):
    token_count = tokens.shape[0]
    sequences = token_count // PROP
    local_heads = w_query.shape[1] // KDIM
    widened = tokens.astype(jnp.float32)
    squares_local = jnp.sum(widened * widened, axis=1, keepdims=True)
    scaled = (widened * norm_gain[None, :]).astype(jnp.bfloat16)
    part_query = jnp.dot(scaled, w_query, preferred_element_type=jnp.float32)
    part_key = jnp.dot(scaled, w_key, preferred_element_type=jnp.float32)
    part_value = jnp.dot(scaled, w_value, preferred_element_type=jnp.float32)
    sum_query, sum_key, sum_value, squares = lax.psum(
        (part_query, part_key, part_value, squares_local), "kv"
    )
    row_scale = lax.rsqrt(squares / D + eps_row)
    queries = (row_scale * sum_query).astype(jnp.bfloat16)
    new_keys = (row_scale * sum_key).astype(jnp.bfloat16)
    new_values = (row_scale * sum_value).astype(jnp.bfloat16)
    query_pairs = queries.reshape(sequences, PROP, local_heads, 2, HEAD)
    key_pairs = new_keys.reshape(sequences, PROP, local_heads, 2, HEAD)
    keys_fresh = new_keys.reshape(sequences, PROP, local_heads, KDIM)
    values_fresh = new_values.reshape(sequences, PROP, local_heads, KDIM)
    cache_positions = cache_keys.shape[1]
    positions = lax.axis_index("kv") * cache_positions + jnp.arange(
        cache_positions, dtype=jnp.int32
    )
    limits = lengths + accepted
    usable = (positions[None, :] < limits[:, None])[:, None, None, None, :]
    score_scale = HEAD ** (-0.5)
    stored_pairs = cache_keys.reshape(sequences, cache_positions, local_heads, 2, HEAD)
    scores = (
        jnp.einsum(
            "bjhmd,bphmd->bjhmp", query_pairs, stored_pairs, preferred_element_type=jnp.float32
        )
        * score_scale
    )
    cache_part = softmax_block(scores, usable, cache_values)
    reachable = jax.vmap(ancestry)(parents) > 0.5
    tree_scores = (
        jnp.einsum("bjhmd,bihmd->bjhmi", query_pairs, key_pairs, preferred_element_type=jnp.float32)
        * score_scale
    )
    tree_part = softmax_block(tree_scores, reachable[:, :, None, None, :], values_fresh)
    own_rows = token_count // lax.axis_size("kv")
    first_row = lax.axis_index("kv") * own_rows
    arrived_max, arrived_totals, arrived_sums = (
        lax.all_to_all(
            leading(cache_part[0], token_count), "kv", split_axis=1, concat_axis=0, tiled=True
        ),
        lax.all_to_all(
            leading(cache_part[1], token_count), "kv", split_axis=1, concat_axis=0, tiled=True
        ),
        lax.all_to_all(
            leading(cache_part[2], token_count), "kv", split_axis=1, concat_axis=0, tiled=True
        ),
    )
    highest = jnp.max(arrived_max, axis=0)
    factors = jnp.exp(arrived_max - highest[None])
    folded = (
        highest,
        jnp.sum(arrived_totals * factors, axis=0),
        jnp.sum(arrived_sums * factors[..., None], axis=0),
    )
    own_tree = tuple(
        (
            lax.dynamic_slice_in_dim(
                member.reshape((token_count,) + member.shape[2:]), first_row, own_rows, 0
            )
            for member in tree_part
        )
    )
    finished = finish(combine(folded, own_tree), lambdas, head_gain).reshape(
        own_rows, local_heads * KDIM
    )
    normed = lax.all_gather(finished, "kv", axis=0, tiled=True)
    layer_out = lax.psum_scatter(
        jnp.dot(normed, w_out, preferred_element_type=jnp.float32).astype(jnp.bfloat16),
        "tp",
        scatter_dimension=0,
        tiled=True,
    )
    slot_of = positions[None, :, None] - limits[:, None, None]
    placing = (slot_of == jnp.arange(PROP, dtype=jnp.int32)[None, None, :]).astype(jnp.bfloat16)
    written = (jnp.sum(placing.astype(jnp.float32), axis=2) > 0.5)[:, :, None, None]
    placed_keys = jnp.einsum(
        "bpj,bjhd->bphd", placing, keys_fresh, preferred_element_type=jnp.float32
    ).astype(jnp.bfloat16)
    placed_values = jnp.einsum(
        "bpj,bjhd->bphd", placing, values_fresh, preferred_element_type=jnp.float32
    ).astype(jnp.bfloat16)
    keys_out = jnp.where(written, placed_keys, cache_keys)
    values_out = jnp.where(written, placed_values, cache_values)
    return (layer_out, keys_out, values_out)


def solution(mesh):
    return jax.shard_map(
        body,
        mesh=mesh,
        in_specs=(
            P(None, "kv"),
            P("kv"),
            P("kv", "tp"),
            P("kv", "tp"),
            P("kv", "tp"),
            P("tp"),
            P(),
            P("tp", "kv"),
            P(None, "kv", "tp", None),
            P(None, "kv", "tp", None),
            P(),
            P(),
            P(),
        ),
        out_specs=(P("tp", "kv"), P(None, "kv", "tp", None), P(None, "kv", "tp", None)),
        check_vma=False,
    )
```

profile of v0, /device:TPU:0, one launch (start us, length us, event | category | flops | bytes accessed | tf_op | source)
XLA Modules:
  0.0 199.4 jit_solution(11030734350312015369)
XLA Ops:
  7.2 1.1 copy-done
  8.4 1.9 fusion.40
  10.2 2.1 %fusion.42 = f32[128,512]{1,0:T(8,128)} fusion(bf16[512,512]{1,0:T(8,128)(2,1)} %param.16, bf16[128,512]{1,0:T(8,128)(2,1)} %param.13, f32[512]{0:T(512)} %param.14), kind=kOutput, calls=%fused_computation.56 | convolution fusion | flops 67305472 | bytes 919552 | tf_op jit(solution)/shard_map/dot_general | solution.py:87
  12.3 1.9 fusion.44
  14.3 23.6 %psum.28 = f32[128,1]{0,1:T(1,128)S(1)} all-reduce(f32[128,1]{0,1:T(1,128)S(1)} %bitcast.101), channel_id=1, replica_groups=mesh['kv'=8,'tp'=4] {'kv'}, use_global_device_ids=true, to_apply=%region_1.0 | all-reduce | flops 128 | bytes 1024 | tf_op jit(solution)/shard_map/psum | solution.py:89
  38.0 7.5 %copy.156 = bf16[8,512,4,128]{1,3,2,0:T(8,128)(2,1)} copy(bf16[8,512,4,128]{3,2,1,0:T(4,128)(2,1)} %param.21) | data formatting | bytes 8388608 | tf_op args[8]
  46.6 0.7 broadcast_bitcast_fusion
  47.4 0.6 broadcast_compare_fusion
  48.0 44.8 %all-reduce.3.cloned.1.call-done = (f32[128,512]{1,0:T(8,128)}, f32[128,512]{1,0:T(8,128)}, f32[128,512]{1,0:T(8,128)}) async-done(((f32[128,512]{1,0:T(8,128)}, f32[128,512]{1,0:T(8,128)}, f32[128,512]{1,0:T(8,128)}), (f32[128,512]{1,0:T(8,128)}, f32[128,512]{1,0:T(8,128)}, f32[128,512]{1,0:T(8,128)})) %all-reduce.3.cloned.1.call-update) | async-done | bytes 786448 | tf_op jit(solution)/shard_map/psum | solution.py:89
  92.8 1.2 multiply_convert_fusion
  94.2 3.0 %bitcast_reduce_fusion = (f32[8,16,4,2]{1,3,2,0:T(2,128)S(1)}, f32[8,4,2,16,512]{4,3,2,1,0:T(8,128)S(1)}) fusion(pred[8,512]{1,0:T(8,128)(4,1)S(1)} %broadcast_compare_fusion.1, bf16[8,512,4,2,64]{1,4,3,2,0:T(8,128)(2,1)} %bitcast.84, bf16[8,16,4,2,64]{4,3,2,1,0:T(2,128)(2,1)S(1)} %reshape.160), kind=kOutput, calls=%fused_computation.5 | convolution fusion | flops 68680704 | bytes 6430720 | tf_op jit(solution)/shard_map/bjhmd,bphmd->bjhmp/dot_general | solution.py:109
  97.2 0.7 fusion.4
  98.2 0.8 reshape.183
  99.0 3.9 %all-to-all-start.2 = ((f32[8,1,128]{2,1,0:T(1,128)}), f32[8,1,128]{2,1,0:T(1,128)}, u32[]{:S(2)}, u32[]{:S(2)}) async-start(f32[8,1,128]{2,1,0:T(1,128)} %reshape.183), calls=%async_computation.2 | async-start | bytes 8192 | tf_op jit(solution)/shard_map/all_to_all | solution.py:127
  103.1 4.0 %fusion.6 = f32[8,16,4,2,128]{4,1,3,2,0:T(8,128)} fusion(bf16[8,512,4,128,1]{3,2,1,0,4:T(4,128)(2,1)} %bitcast.102, f32[8,4,2,16,512]{4,3,2,1,0:T(8,128)S(1)} %get-tuple-element.41, f32[8,16,4,2]{1,3,2,0:T(2,128)S(1)} %get-tuple-element.40, pred[8,512]{1,0:T(8,128)(4,1)S(1)} %broadcast_compare_fusion.1), kind=kOutput, calls=%fused_computation.12 | convolution fusion | flops 136839168 | bytes 6823936 | tf_op jit(solution)/shard_map/bjhmp,bphd->bjhmd/dot_general | solution.py:44
  108.0 0.8 reshape.181
  109.3 5.4 %all-to-all-start.1 = ((f32[8,1,128]{2,1,0:T(1,128)}), f32[8,1,128]{2,1,0:T(1,128)S(1)}, u32[]{:S(2)}, u32[]{:S(2)}) async-start(f32[8,1,128]{2,1,0:T(1,128)} %reshape.181), calls=%async_computation.1 | async-start | bytes 8192 | tf_op jit(solution)/shard_map/all_to_all | solution.py:124
  114.9 1.0 copy.200
  116.3 1.2 copy.160
  117.5 3.6 %all-to-all-done.1 = f32[8,1,128]{2,1,0:T(1,128)S(1)} async-done(((f32[8,1,128]{2,1,0:T(1,128)}), f32[8,1,128]{2,1,0:T(1,128)S(1)}, u32[]{:S(2)}, u32[]{:S(2)}) %all-to-all-start.1) | async-done | bytes 4128 | tf_op jit(solution)/shard_map/all_to_all | solution.py:124
  121.2 3.5 %all-to-all-start = ((f32[1,128,4,2,128]{4,3,2,0,1:T(2,128)}), f32[1,128,4,2,128]{4,3,2,0,1:T(2,128)S(1)}, u32[]{:S(2)}, u32[]{:S(2)}) async-start(f32[1,128,4,2,128]{4,3,2,0,1:T(2,128)} %copy.160), calls=%async_computation | async-start | bytes 1048576 | tf_op jit(solution)/shard_map/all_to_all | solution.py:130
  124.9 3.6 %copy_select_fusion.1 = bf16[8,512,4,128]{3,1,2,0:T(8,128)(2,1)S(1)} fusion(bf16[8,512,4,128]{3,2,1,0:T(4,128)(2,1)} %param.21, pred[8,512]{1,0:T(8,128)(4,1)S(1)} %copy-done.12, bf16[8,16,4,128]{3,2,1,0:T(4,128)(2,1)S(1)} %reshape.170, s32[8,512]{1,0:T(8,128)S(1)} %copy-done.8), kind=kOutput, calls=%fused_computation.3 | convolution fusion | flops 71368704 | bytes 8540160 | tf_op jit(solution)/shard_map/bpj,bjhd->bphd/dot_general | solution.py:162
  128.5 5.3 %copy.189 = bf16[8,512,4,128]{3,2,1,0:T(4,128)(2,1)} copy(bf16[8,512,4,128]{3,1,2,0:T(8,128)(2,1)S(1)} %copy_select_fusion.1) | data formatting | bytes 8388608
  134.3 0.7 reduce.5
  135.7 1.3 reduce.4
  137.9 0.8 multiply_add_fusion
  138.7 0.7 multiply_reduce_fusion
  140.2 30.8 %all_gather.3 = bf16[128,512]{1,0:T(8,128)(2,1)S(1)} all-gather(bf16[16,512]{1,0:T(8,128)(2,1)S(1)} %fusion.53), channel_id=1, replica_groups=mesh['kv'=8,'tp'=4] {'kv'}, dimensions={0}, use_global_device_ids=true | all-gather | bytes 147456 | tf_op jit(solution)/shard_map/all_gather | solution.py:152
  171.0 0.9 convolution_convert_fusion
  171.9 3.5 %copy_select_fusion = bf16[8,512,4,128]{3,1,2,0:T(8,128)(2,1)S(1)} fusion(bf16[8,512,4,128]{3,2,1,0:T(4,128)(2,1)} %param.22, pred[8,512]{1,0:T(8,128)(4,1)S(1)} %copy-done.12, bf16[8,16,4,128]{3,2,1,0:T(4,128)(2,1)S(1)} %reshape.166, s32[8,512]{1,0:T(8,128)S(1)} %copy-done.8), kind=kOutput, calls=%fused_computation.2 | convolution fusion | flops 71368704 | bytes 8540160 | tf_op jit(solution)/shard_map/bpj,bjhd->bphd/dot_general | solution.py:165
  175.5 5.3 %copy.190 = bf16[8,512,4,128]{3,2,1,0:T(4,128)(2,1)} copy(bf16[8,512,4,128]{3,1,2,0:T(8,128)(2,1)S(1)} %copy_select_fusion) | data formatting | bytes 8388608
  180.7 11.8 %reduce-scatter.2.cloned.1.call-done = bf16[32,512]{1,0:T(8,128)(2,1)} async-done(((bf16[128,512]{1,0:T(8,128)(2,1)}), bf16[32,512]{1,0:T(8,128)(2,1)}) %reduce-scatter.2.cloned.1.call-update) | async-done | bytes 32784 | tf_op jit(solution)/shard_map/reduce_scatter | solution.py:153
  (84 shorter events, 7.0 us)
Async XLA Ops:
  7.2 1.2 copy-start
  7.2 7.0 %copy-start.1 = (bf16[128,512]{1,0:T(8,128)(2,1)S(1)}, bf16[128,512]{1,0:T(8,128)(2,1)}, u32[]{:S(2)}) copy-start(bf16[128,512]{1,0:T(8,128)(2,1)} %param.13) | copy-start | bytes 393220
  7.2 5.1 %copy-start.2 = (bf16[512,512]{1,0:T(8,128)(2,1)S(1)}, bf16[512,512]{1,0:T(8,128)(2,1)}, u32[]{:S(2)}) copy-start(bf16[512,512]{1,0:T(8,128)(2,1)} %param.15) | copy-start | bytes 1572868
  7.2 85.6 %all-reduce.3.cloned.1.call-start = ((), (), s32[]{:S(2)}) async-start(), calls=%async_computation.5 | async-start | bytes 1572864 | tf_op jit(solution)/shard_map/psum | solution.py:89
  38.0 7.5 %copy-start.11 = (s32[8,16]{1,0:T(8,128)S(1)}, s32[8,16]{1,0:T(8,128)}, u32[]{:S(2)}) copy-start(s32[8,16]{1,0:T(8,128)} %param.25) | copy-start | bytes 1540
  38.0 8.5 %copy-start.16 = (s32[8]{0:T(128)S(1)}, s32[8]{0:T(128)}, u32[]{:S(2)}) copy-start(s32[8]{0:T(128)} %param.23) | copy-start | bytes 100
  38.0 8.5 %copy-start.17 = (s32[8]{0:T(128)S(1)}, s32[8]{0:T(128)}, u32[]{:S(2)}) copy-start(s32[8]{0:T(128)} %param.24) | copy-start | bytes 100
  38.0 8.6 %copy-start.13 = (f32[4]{0:T(128)S(1)}, f32[4]{0:T(128)}, u32[]{:S(2)}) copy-start(f32[4]{0:T(128)} %param.18) | copy-start | bytes 52
  38.0 8.6 %copy-start.15 = (f32[128]{0:T(128)S(1)}, f32[128]{0:T(128)}, u32[]{:S(2)}) copy-start(f32[128]{0:T(128)} %param.19) | copy-start | bytes 1540
  46.5 47.7 %copy-start.7 = (s32[8,512]{1,0:T(8,128)}, s32[8,512]{1,0:T(8,128)S(1)}, u32[]{:S(2)}) copy-start(s32[8,512]{1,0:T(8,128)S(1)} %broadcast_subtract_fusion) | copy-start | bytes 49156
  97.2 9.9 %copy-start.5 = (f32[8,16,4,2]{1,3,2,0:T(2,128)}, f32[8,16,4,2]{1,3,2,0:T(2,128)S(1)}, u32[]{:S(2)}) copy-start(f32[8,16,4,2]{1,3,2,0:T(2,128)S(1)} %get-tuple-element.40) | copy-start | bytes 12292
  99.0 10.3 %all-to-all-start.2 = ((f32[8,1,128]{2,1,0:T(1,128)}), f32[8,1,128]{2,1,0:T(1,128)}, u32[]{:S(2)}, u32[]{:S(2)}) async-start(f32[8,1,128]{2,1,0:T(1,128)} %reshape.183), calls=%async_computation.2 | async-start | bytes 8192 | tf_op jit(solution)/shard_map/all_to_all | solution.py:127
  107.1 0.8 copy-start.6
  107.1 9.1 %copy-start.4 = (f32[8,16,4,2,128]{4,1,3,2,0:T(8,128)S(1)}, f32[8,16,4,2,128]{4,1,3,2,0:T(8,128)}, u32[]{:S(2)}) copy-start(f32[8,16,4,2,128]{4,1,3,2,0:T(8,128)} %fusion.6) | copy-start | bytes 1572868
  109.3 11.9 %all-to-all-start.1 = ((f32[8,1,128]{2,1,0:T(1,128)}), f32[8,1,128]{2,1,0:T(1,128)S(1)}, u32[]{:S(2)}, u32[]{:S(2)}) async-start(f32[8,1,128]{2,1,0:T(1,128)} %reshape.181), calls=%async_computation.1 | async-start | bytes 8192 | tf_op jit(solution)/shard_map/all_to_all | solution.py:124
  116.2 8.7 %copy-start.8 = (s32[8,512]{1,0:T(8,128)S(1)}, s32[8,512]{1,0:T(8,128)}, u32[]{:S(2)}) copy-start(s32[8,512]{1,0:T(8,128)} %copy-done.7) | copy-start | bytes 49156
  116.2 8.7 %copy-start.12 = (pred[8,512]{1,0:T(8,128)(4,1)S(1)}, pred[8,512]{1,0:T(8,128)(4,1)}, u32[]{:S(2)}) copy-start(pred[8,512]{1,0:T(8,128)(4,1)} %broadcast_compare_fusion) | copy-start | bytes 12292
  121.2 17.6 %all-to-all-start = ((f32[1,128,4,2,128]{4,3,2,0,1:T(2,128)}), f32[1,128,4,2,128]{4,3,2,0,1:T(2,128)S(1)}, u32[]{:S(2)}, u32[]{:S(2)}) async-start(f32[1,128,4,2,128]{4,3,2,0,1:T(2,128)} %copy.160), calls=%async_computation | async-start | bytes 1048576 | tf_op jit(solution)/shard_map/all_to_all | solution.py:130
  124.7 67.9 %reduce-scatter.2.cloned.1.call-start = ((), (), s32[]{:S(2)}) async-start(), calls=%async_computation.4 | async-start | bytes 163840 | tf_op jit(solution)/shard_map/reduce_scatter | solution.py:153
  133.7 6.1 %copy-start.14 = (f32[4]{0:T(128)S(1)}, f32[4]{0:T(128)}, u32[]{:S(2)}) copy-start(f32[4]{0:T(128)} %param.18) | copy-start | bytes 52
  133.7 6.4 %copy-start.9 = (f32[512]{0:T(512)S(1)}, f32[512]{0:T(512)}, u32[]{:S(2)}) copy-start(f32[512]{0:T(512)} %get-tuple-element.42) | copy-start | bytes 6148
  133.7 6.4 %copy-start.10 = (f32[512]{0:T(512)S(1)}, f32[512]{0:T(512)}, u32[]{:S(2)}) copy-start(f32[512]{0:T(512)} %get-tuple-element.43) | copy-start | bytes 6148
  133.7 37.3 %copy-start.3 = (bf16[512,512]{1,0:T(8,128)(2,1)S(1)}, bf16[512,512]{1,0:T(8,128)(2,1)}, u32[]{:S(2)}) copy-start(bf16[512,512]{1,0:T(8,128)(2,1)} %param.20) | copy-start | bytes 1572868
Sparse Core Ops, SparseCore 0:
  14.3 78.4 all-reduce.2
  172.0 20.4 reduce-scatter.1
where the time goes:
time: 200 us; the launch traced here: 199 us
  waiting for transfers between devices  60.8 us (30%)
  blocking collectives  54.5 us (27%)
  local copies, waits for them, and re-layouts  27.1 us (14%)
  matrix products  22.2 us (11%)
  between operations  14.5 us (7%)
  starting transfers between devices  13.1 us (7%)
  other arithmetic  7.19 us (4%)
    psum x1, waiting for transfers between devices, body(): lax.psum((part_query, part_key, part_value, squares_local), 'kv')  44.8 us
    all_gather x1, blocking collectives, body(): normed = lax.all_gather(finished, 'kv', axis=0, tiled=True)  30.8 us
    psum x1, blocking collectives, body(): lax.psum((part_query, part_key, part_value, squares_local), 'kv')  23.6 us
    unnamed x45, local copies, waits for them, and re-layouts  21.6 us
    reduce_scatter x1, waiting for transfers between devices, body(): lax.psum_scatter(jnp.dot(normed, w_out, preferred_element_type=jnp.float3...  11.8 us
    all_to_all x1, starting transfers between devices, body(): lax.all_to_all(leading(cache_part[0], token_count), 'kv', split_axis=1, c...  5.43 us
    dot_general x2, matrix products, softmax_block(): jnp.einsum('bjhmp,bphd->bjhmd', weights.astype(jnp.bfloat16), values, pre...  4.32 us
  transfers between devices with their start and end apart: 5, of which 4 were waited for; matrix products, arithmetic and copies ran while one was open for 21% of the time, Pallas kernels for 0%

commit v1 on v0

--- a/solution.py
+++ b/solution.py
@@ -10,6 +10,17 @@
 eps_row = 1e-06
 eps_head = 1e-05
 masked = -1e30
+
+
+def gather_by_hops(shard, axis, dim):
+    size = lax.axis_size(axis)
+    right = [(i, (i + 1) % size) for i in range(size)]
+    parts = [shard]
+    for far in range(1, size):
+        parts = [lax.ppermute(parts[0], axis, right), *parts]
+    whole = jnp.concatenate(parts, axis=dim)
+    offset = (lax.axis_index(axis) + 1) * parts[-1].shape[dim]
+    return jnp.roll(whole, offset, axis=dim)
 
 
 def ancestry(parents):
@@ -149,7 +160,7 @@
     finished = finish(combine(folded, own_tree), lambdas, head_gain).reshape(
         own_rows, local_heads * KDIM
     )
-    normed = lax.all_gather(finished, "kv", axis=0, tiled=True)
+    normed = gather_by_hops(finished, "kv", 0)
     layer_out = lax.psum_scatter(
         jnp.dot(normed, w_out, preferred_element_type=jnp.float32).astype(jnp.bfloat16),
         "tp",

time: 200 us -> 214 us (1.070)
  waiting for transfers between devices: 60.8 us -> 109 us
  blocking collectives: 54.5 us -> 23.3 us
    ppermute x0 -> x7, waiting for transfers between devices: none -> 36.9 us  [gather_by_hops(): parts = [lax.ppermute(parts[0], axis, right), *parts]]
    all_gather x1 -> x0, blocking collectives: 30.8 us -> none  [body(): normed = lax.all_gather(finished, 'kv', axis=0, tiled=True)]
    all_to_all x1, waiting for transfers between devices: 0.01 us -> 7.21 us  [body(): lax.all_to_all(leading(cache_part[2], token_count), 'kv', split_axis=1, c...]
    unnamed x45 -> x44, local copies, waits for them, and re-layouts: 21.6 us -> 21.5 us
  transfers between devices with their start and end apart: 5 -> 12, of which waited for: 4 -> 11; matrix products, arithmetic and copies ran while one was open for 21% -> 18% of each run, Pallas kernels for 0% -> 0%
where the time goes in v1:
time: 214 us
  waiting for transfers between devices  109 us (51%)
  local copies, waits for them, and re-layouts  25.8 us (12%)
  blocking collectives  23.3 us (11%)
  matrix products  22.3 us (10%)
  between operations  14.6 us (7%)
  starting transfers between devices  13.8 us (6%)
  other arithmetic  5.18 us (2%)
    psum x1, waiting for transfers between devices, body(): lax.psum((part_query, part_key, part_value, squares_local), 'kv')  46.5 us
    ppermute x7, waiting for transfers between devices, gather_by_hops(): parts = [lax.ppermute(parts[0], axis, right), *parts]  36.9 us
    psum x1, blocking collectives, body(): lax.psum((part_query, part_key, part_value, squares_local), 'kv')  23.3 us
    unnamed x44, local copies, waits for them, and re-layouts  21.5 us
    reduce_scatter x1, waiting for transfers between devices, body(): lax.psum_scatter(jnp.dot(normed, w_out, preferred_element_type=jnp.float3...  12.4 us
    all_to_all x1, waiting for transfers between devices, body(): lax.all_to_all(leading(cache_part[2], token_count), 'kv', split_axis=1, c...  7.21 us
    all_to_all x1, starting transfers between devices, body(): lax.all_to_all(leading(cache_part[0], token_count), 'kv', split_axis=1, c...  4.87 us
    all_to_all x1, waiting for transfers between devices, body(): lax.all_to_all(leading(cache_part[0], token_count), 'kv', split_axis=1, c...  4.57 us
  transfers between devices with their start and end apart: 12, of which 11 were waited for; matrix products, arithmetic and copies ran while one was open for 18% of the time, Pallas kernels for 0%

profile of v1, /device:TPU:0, one launch (start us, length us, event | category | flops | bytes accessed | tf_op | source)
XLA Modules:
  0.0 213.6 jit_solution(17452914201273674330)
XLA Ops:
  7.3 1.1 copy-done
  8.4 1.9 fusion.41
  10.2 2.1 fusion.43
  12.3 1.9 fusion.45
  15.3 7.4 %copy.156 = bf16[8,512,4,128]{1,3,2,0:T(8,128)(2,1)} copy(bf16[8,512,4,128]{3,2,1,0:T(4,128)(2,1)} %param.21) | data formatting | bytes 8388608 | tf_op args[8]
  22.8 23.3 %psum.28 = f32[128,1]{0,1:T(1,128)S(1)} all-reduce(f32[128,1]{0,1:T(1,128)S(1)} %bitcast.100), channel_id=1, replica_groups=mesh['kv'=8,'tp'=4] {'kv'}, use_global_device_ids=true, to_apply=%region_1.0 | all-reduce | flops 128 | bytes 1024 | tf_op jit(solution)/shard_map/psum | solution.py:100
  46.3 46.5 %all-reduce.3.cloned.1.call-done = (f32[128,512]{1,0:T(8,128)}, f32[128,512]{1,0:T(8,128)}, f32[128,512]{1,0:T(8,128)}) async-done(((f32[128,512]{1,0:T(8,128)}, f32[128,512]{1,0:T(8,128)}, f32[128,512]{1,0:T(8,128)}), (f32[128,512]{1,0:T(8,128)}, f32[128,512]{1,0:T(8,128)}, f32[128,512]{1,0:T(8,128)})) %all-reduce.3.cloned.1.call-update) | async-done | bytes 786448 | tf_op jit(solution)/shard_map/psum | solution.py:100
  92.8 1.2 multiply_convert_fusion
  94.2 3.0 %bitcast_reduce_fusion = (f32[8,16,4,2]{1,3,2,0:T(2,128)S(1)}, f32[8,4,2,16,512]{4,3,2,1,0:T(8,128)S(1)}) fusion(pred[8,512]{1,0:T(8,128)(4,1)S(1)} %broadcast_compare_fusion.1, bf16[8,512,4,2,64]{1,4,3,2,0:T(8,128)(2,1)} %bitcast.83, bf16[8,16,4,2,64]{4,3,2,1,0:T(2,128)(2,1)S(1)} %reshape.160), kind=kOutput, calls=%fused_computation.5 | convolution fusion | flops 68680704 | bytes 6430720 | tf_op jit(solution)/shard_map/bjhmd,bphmd->bjhmp/dot_general | solution.py:120
  98.2 0.8 reshape.183
  99.0 3.8 %all-to-all-start.2 = ((f32[8,1,128]{2,1,0:T(1,128)}), f32[8,1,128]{2,1,0:T(1,128)S(1)}, u32[]{:S(2)}, u32[]{:S(2)}) async-start(f32[8,1,128]{2,1,0:T(1,128)} %reshape.183), calls=%async_computation.2 | async-start | bytes 8192 | tf_op jit(solution)/shard_map/all_to_all | solution.py:138
  102.7 4.1 %fusion.6 = f32[8,16,4,2,128]{4,1,3,2,0:T(8,128)} fusion(bf16[8,512,4,128,1]{3,2,1,0,4:T(4,128)(2,1)} %bitcast.101, f32[8,4,2,16,512]{4,3,2,1,0:T(8,128)S(1)} %get-tuple-element.41, f32[8,16,4,2]{1,3,2,0:T(2,128)S(1)} %get-tuple-element.40, pred[8,512]{1,0:T(8,128)(4,1)S(1)} %broadcast_compare_fusion.1), kind=kOutput, calls=%fused_computation.12 | convolution fusion | flops 136839168 | bytes 6823936 | tf_op jit(solution)/shard_map/bjhmp,bphd->bjhmd/dot_general | solution.py:55
  107.0 0.8 reshape.181
  108.0 1.2 all-to-all-done.2
  109.1 4.9 %all-to-all-start.1 = ((f32[8,1,128]{2,1,0:T(1,128)}), f32[8,1,128]{2,1,0:T(1,128)S(1)}, u32[]{:S(2)}, u32[]{:S(2)}) async-start(f32[8,1,128]{2,1,0:T(1,128)} %reshape.181), calls=%async_computation.1 | async-start | bytes 8192 | tf_op jit(solution)/shard_map/all_to_all | solution.py:135
  114.7 1.2 copy.160
  115.9 4.6 %all-to-all-done.1 = f32[8,1,128]{2,1,0:T(1,128)S(1)} async-done(((f32[8,1,128]{2,1,0:T(1,128)}), f32[8,1,128]{2,1,0:T(1,128)S(1)}, u32[]{:S(2)}, u32[]{:S(2)}) %all-to-all-start.1) | async-done | bytes 4128 | tf_op jit(solution)/shard_map/all_to_all | solution.py:135
  120.4 3.5 %all-to-all-start = ((f32[1,128,4,2,128]{4,3,2,0,1:T(2,128)}), f32[1,128,4,2,128]{4,3,2,0,1:T(2,128)S(1)}, u32[]{:S(2)}, u32[]{:S(2)}) async-start(f32[1,128,4,2,128]{4,3,2,0,1:T(2,128)} %copy.160), calls=%async_computation | async-start | bytes 1048576 | tf_op jit(solution)/shard_map/all_to_all | solution.py:141
  128.4 7.2 %all-to-all-done = f32[1,128,4,2,128]{4,3,2,0,1:T(2,128)S(1)} async-done(((f32[1,128,4,2,128]{4,3,2,0,1:T(2,128)}), f32[1,128,4,2,128]{4,3,2,0,1:T(2,128)S(1)}, u32[]{:S(2)}, u32[]{:S(2)}) %all-to-all-start) | async-done | bytes 524320 | tf_op jit(solution)/shard_map/all_to_all | solution.py:141
  137.0 1.6 collective-permute-start
  138.6 4.9 %collective-permute-done = bf16[16,512]{1,0:T(8,128)(2,1)S(1)} collective-permute-done((bf16[16,512]{1,0:T(8,128)(2,1)S(1)}, bf16[16,512]{1,0:T(8,128)(2,1)S(1)}, u32[]{:S(2)}, u32[]{:S(2)}) %collective-permute-start) | collective-permute-done | bytes 16416 | tf_op jit(solution)/shard_map/ppermute | solution.py:20
  143.5 6.4 %collective-permute-done.1 = bf16[16,512]{1,0:T(8,128)(2,1)S(1)} collective-permute-done((bf16[16,512]{1,0:T(8,128)(2,1)S(1)}, bf16[16,512]{1,0:T(8,128)(2,1)S(1)}, u32[]{:S(2)}, u32[]{:S(2)}) %collective-permute-start.1) | collective-permute-done | bytes 16416 | tf_op jit(solution)/shard_map/ppermute | solution.py:20
  150.0 6.4 %collective-permute-done.2 = bf16[16,512]{1,0:T(8,128)(2,1)S(1)} collective-permute-done((bf16[16,512]{1,0:T(8,128)(2,1)S(1)}, bf16[16,512]{1,0:T(8,128)(2,1)S(1)}, u32[]{:S(2)}, u32[]{:S(2)}) %collective-permute-start.2) | collective-permute-done | bytes 16416 | tf_op jit(solution)/shard_map/ppermute | solution.py:20
  156.5 6.4 %collective-permute-done.3 = bf16[16,512]{1,0:T(8,128)(2,1)S(1)} collective-permute-done((bf16[16,512]{1,0:T(8,128)(2,1)S(1)}, bf16[16,512]{1,0:T(8,128)(2,1)S(1)}, u32[]{:S(2)}, u32[]{:S(2)}) %collective-permute-start.3) | collective-permute-done | bytes 16416 | tf_op jit(solution)/shard_map/ppermute | solution.py:20
  162.9 6.4 %collective-permute-done.4 = bf16[16,512]{1,0:T(8,128)(2,1)S(1)} collective-permute-done((bf16[16,512]{1,0:T(8,128)(2,1)S(1)}, bf16[16,512]{1,0:T(8,128)(2,1)S(1)}, u32[]{:S(2)}, u32[]{:S(2)}) %collective-permute-start.4) | collective-permute-done | bytes 16416 | tf_op jit(solution)/shard_map/ppermute | solution.py:20
  169.3 6.4 %collective-permute-done.5 = bf16[16,512]{1,0:T(8,128)(2,1)S(1)} collective-permute-done((bf16[16,512]{1,0:T(8,128)(2,1)S(1)}, bf16[16,512]{1,0:T(8,128)(2,1)S(1)}, u32[]{:S(2)}, u32[]{:S(2)}) %collective-permute-start.5) | collective-permute-done | bytes 16416 | tf_op jit(solution)/shard_map/ppermute | solution.py:20
  175.7 3.5 %copy_select_fusion.1 = bf16[8,512,4,128]{3,1,2,0:T(8,128)(2,1)S(1)} fusion(bf16[8,512,4,128]{3,2,1,0:T(4,128)(2,1)} %param.21, pred[8,512]{1,0:T(8,128)(4,1)S(1)} %broadcast_compare_fusion, bf16[8,16,4,128]{3,2,1,0:T(4,128)(2,1)S(1)} %reshape.170, s32[8,512]{1,0:T(8,128)S(1)} %broadcast_subtract_fusion), kind=kOutput, calls=%fused_computation.3 | convolution fusion | flops 71368704 | bytes 8540160 | tf_op jit(solution)/shard_map/bpj,bjhd->bphd/dot_general | solution.py:173
  179.3 5.3 %copy.189 = bf16[8,512,4,128]{3,2,1,0:T(4,128)(2,1)} copy(bf16[8,512,4,128]{3,1,2,0:T(8,128)(2,1)S(1)} %copy_select_fusion.1) | data formatting | bytes 8388608
  184.7 0.9 convolution_convert_fusion
  185.6 3.6 %copy_select_fusion = bf16[8,512,4,128]{3,1,2,0:T(8,128)(2,1)S(1)} fusion(bf16[8,512,4,128]{3,2,1,0:T(4,128)(2,1)} %param.22, pred[8,512]{1,0:T(8,128)(4,1)S(1)} %broadcast_compare_fusion, bf16[8,16,4,128]{3,2,1,0:T(4,128)(2,1)S(1)} %reshape.166, s32[8,512]{1,0:T(8,128)S(1)} %broadcast_subtract_fusion), kind=kOutput, calls=%fused_computation.2 | convolution fusion | flops 71368704 | bytes 8540160 | tf_op jit(solution)/shard_map/bpj,bjhd->bphd/dot_general | solution.py:176
  189.2 5.3 %copy.190 = bf16[8,512,4,128]{3,2,1,0:T(4,128)(2,1)} copy(bf16[8,512,4,128]{3,1,2,0:T(8,128)(2,1)S(1)} %copy_select_fusion) | data formatting | bytes 8388608
  194.4 12.4 %reduce-scatter.2.cloned.1.call-done = bf16[32,512]{1,0:T(8,128)(2,1)} async-done(((bf16[128,512]{1,0:T(8,128)(2,1)}), bf16[32,512]{1,0:T(8,128)(2,1)}) %reduce-scatter.2.cloned.1.call-update) | async-done | bytes 32784 | tf_op jit(solution)/shard_map/reduce_scatter | solution.py:164
  (97 shorter events, 9.5 us)
Async XLA Ops:
  7.2 1.2 copy-start
  7.2 7.9 %copy-start.1 = (bf16[128,512]{1,0:T(8,128)(2,1)S(1)}, bf16[128,512]{1,0:T(8,128)(2,1)}, u32[]{:S(2)}) copy-start(bf16[128,512]{1,0:T(8,128)(2,1)} %param.13) | copy-start | bytes 393220
  7.2 5.1 %copy-start.2 = (bf16[512,512]{1,0:T(8,128)(2,1)S(1)}, bf16[512,512]{1,0:T(8,128)(2,1)}, u32[]{:S(2)}) copy-start(bf16[512,512]{1,0:T(8,128)(2,1)} %param.15) | copy-start | bytes 1572868
  7.2 7.0 %copy-start.5 = (s32[8,16]{1,0:T(8,128)S(1)}, s32[8,16]{1,0:T(8,128)}, u32[]{:S(2)}) copy-start(s32[8,16]{1,0:T(8,128)} %param.25) | copy-start | bytes 1540
  7.2 85.6 %all-reduce.3.cloned.1.call-start = ((), (), s32[]{:S(2)}) async-start(), calls=%async_computation.5 | async-start | bytes 1572864 | tf_op jit(solution)/shard_map/psum | solution.py:100
  15.2 7.6 %copy-start.8 = (s32[8]{0:T(128)S(1)}, s32[8]{0:T(128)}, u32[]{:S(2)}) copy-start(s32[8]{0:T(128)} %param.23) | copy-start | bytes 100
  15.2 7.6 %copy-start.9 = (s32[8]{0:T(128)S(1)}, s32[8]{0:T(128)}, u32[]{:S(2)}) copy-start(s32[8]{0:T(128)} %param.24) | copy-start | bytes 100
  15.2 30.9 %copy-start.6 = (f32[4]{0:T(128)S(1)}, f32[4]{0:T(128)}, u32[]{:S(2)}) copy-start(f32[4]{0:T(128)} %param.18) | copy-start | bytes 52
  15.2 30.9 %copy-start.7 = (f32[128]{0:T(128)S(1)}, f32[128]{0:T(128)}, u32[]{:S(2)}) copy-start(f32[128]{0:T(128)} %param.19) | copy-start | bytes 1540
  99.0 10.2 %all-to-all-start.2 = ((f32[8,1,128]{2,1,0:T(1,128)}), f32[8,1,128]{2,1,0:T(1,128)S(1)}, u32[]{:S(2)}, u32[]{:S(2)}) async-start(f32[8,1,128]{2,1,0:T(1,128)} %reshape.183), calls=%async_computation.2 | async-start | bytes 8192 | tf_op jit(solution)/shard_map/all_to_all | solution.py:138
  106.8 7.8 %copy-start.4 = (f32[8,16,4,2,128]{4,1,3,2,0:T(8,128)S(1)}, f32[8,16,4,2,128]{4,1,3,2,0:T(8,128)}, u32[]{:S(2)}) copy-start(f32[8,16,4,2,128]{4,1,3,2,0:T(8,128)} %fusion.6) | copy-start | bytes 1572868
  109.1 11.3 %all-to-all-start.1 = ((f32[8,1,128]{2,1,0:T(1,128)}), f32[8,1,128]{2,1,0:T(1,128)S(1)}, u32[]{:S(2)}, u32[]{:S(2)}) async-start(f32[8,1,128]{2,1,0:T(1,128)} %reshape.181), calls=%async_computation.1 | async-start | bytes 8192 | tf_op jit(solution)/shard_map/all_to_all | solution.py:135
  120.4 15.2 %all-to-all-start = ((f32[1,128,4,2,128]{4,3,2,0,1:T(2,128)}), f32[1,128,4,2,128]{4,3,2,0,1:T(2,128)S(1)}, u32[]{:S(2)}, u32[]{:S(2)}) async-start(f32[1,128,4,2,128]{4,3,2,0,1:T(2,128)} %copy.160), calls=%async_computation | async-start | bytes 1048576 | tf_op jit(solution)/shard_map/all_to_all | solution.py:141
  123.9 82.9 %reduce-scatter.2.cloned.1.call-start = ((), (), s32[]{:S(2)}) async-start(), calls=%async_computation.4 | async-start | bytes 163840 | tf_op jit(solution)/shard_map/reduce_scatter | solution.py:164
  137.0 6.5 %collective-permute-start = (bf16[16,512]{1,0:T(8,128)(2,1)S(1)}, bf16[16,512]{1,0:T(8,128)(2,1)S(1)}, u32[]{:S(2)}, u32[]{:S(2)}) collective-permute-start(bf16[16,512]{1,0:T(8,128)(2,1)S(1)} %fusion.54), channel_id=1, source_target_pairs={{0,4},{4,8},{8,12},{12,16},{16,20},{20,24},{24,28},{28,0},{1,5},{5... | collective-permute-start | bytes 49160 | tf_op jit(solution)/shard_map/ppermute | solution.py:20
  143.5 6.4 %collective-permute-start.1 = (bf16[16,512]{1,0:T(8,128)(2,1)S(1)}, bf16[16,512]{1,0:T(8,128)(2,1)S(1)}, u32[]{:S(2)}, u32[]{:S(2)}) collective-permute-start(bf16[16,512]{1,0:T(8,128)(2,1)S(1)} %collective-permute-done), channel_id=1, source_target_pairs={{0,4},{4,8},{8,12},{12,16},{16,20},{20,24},{24,28},{28,0},{1,5},{5... | collective-permute-start | bytes 49160 | tf_op jit(solution)/shard_map/ppermute | solution.py:20
  150.0 6.4 %collective-permute-start.2 = (bf16[16,512]{1,0:T(8,128)(2,1)S(1)}, bf16[16,512]{1,0:T(8,128)(2,1)S(1)}, u32[]{:S(2)}, u32[]{:S(2)}) collective-permute-start(bf16[16,512]{1,0:T(8,128)(2,1)S(1)} %collective-permute-done.1), channel_id=1, source_target_pairs={{0,4},{4,8},{8,12},{12,16},{16,20},{20,24},{24,28},{28,0},{1,5},{5... | collective-permute-start | bytes 49160 | tf_op jit(solution)/shard_map/ppermute | solution.py:20
  156.4 6.4 %collective-permute-start.3 = (bf16[16,512]{1,0:T(8,128)(2,1)S(1)}, bf16[16,512]{1,0:T(8,128)(2,1)S(1)}, u32[]{:S(2)}, u32[]{:S(2)}) collective-permute-start(bf16[16,512]{1,0:T(8,128)(2,1)S(1)} %collective-permute-done.2), channel_id=1, source_target_pairs={{0,4},{4,8},{8,12},{12,16},{16,20},{20,24},{24,28},{28,0},{1,5},{5... | collective-permute-start | bytes 49160 | tf_op jit(solution)/shard_map/ppermute | solution.py:20
  162.8 6.4 %collective-permute-start.4 = (bf16[16,512]{1,0:T(8,128)(2,1)S(1)}, bf16[16,512]{1,0:T(8,128)(2,1)S(1)}, u32[]{:S(2)}, u32[]{:S(2)}) collective-permute-start(bf16[16,512]{1,0:T(8,128)(2,1)S(1)} %collective-permute-done.3), channel_id=1, source_target_pairs={{0,4},{4,8},{8,12},{12,16},{16,20},{20,24},{24,28},{28,0},{1,5},{5... | collective-permute-start | bytes 49160 | tf_op jit(solution)/shard_map/ppermute | solution.py:20
  169.3 6.4 %collective-permute-start.5 = (bf16[16,512]{1,0:T(8,128)(2,1)S(1)}, bf16[16,512]{1,0:T(8,128)(2,1)S(1)}, u32[]{:S(2)}, u32[]{:S(2)}) collective-permute-start(bf16[16,512]{1,0:T(8,128)(2,1)S(1)} %collective-permute-done.4), channel_id=1, source_target_pairs={{0,4},{4,8},{8,12},{12,16},{16,20},{20,24},{24,28},{28,0},{1,5},{5... | collective-permute-start | bytes 49160 | tf_op jit(solution)/shard_map/ppermute | solution.py:20
  175.7 8.8 %collective-permute-start.6 = (bf16[16,512]{1,0:T(8,128)(2,1)S(1)}, bf16[16,512]{1,0:T(8,128)(2,1)S(1)}, u32[]{:S(2)}, u32[]{:S(2)}) collective-permute-start(bf16[16,512]{1,0:T(8,128)(2,1)S(1)} %collective-permute-done.5), channel_id=1, source_target_pairs={{0,4},{4,8},{8,12},{12,16},{16,20},{20,24},{24,28},{28,0},{1,5},{5... | collective-permute-start | bytes 49160 | tf_op jit(solution)/shard_map/ppermute | solution.py:20
  179.3 5.4 %copy-start.3 = (bf16[512,512]{1,0:T(8,128)(2,1)S(1)}, bf16[512,512]{1,0:T(8,128)(2,1)}, u32[]{:S(2)}) copy-start(bf16[512,512]{1,0:T(8,128)(2,1)} %param.20) | copy-start | bytes 1572868
Sparse Core Ops, SparseCore 0:
  14.3 78.4 all-reduce.2
  185.7 21.0 reduce-scatter.1
